TPU v7x, 32 devices: a whole 2x2x4 slice. The times are simulated.
32 devices in a mesh: rep: 2 (over x), fs: 4 (over z), tp: 4 (over y, core).
Axes of the slice: x: 2, y: 2, z: 4, core: 2. Of those that a mesh axis runs over, the one named last changes fastest.
Arguments:
- tokens: bfloat16 [4096, 2048], P(('rep', 'fs', 'tp')), may hold values from -6 to 6
- mix_gain: bfloat16 [2048], replicated, may hold values from 0.099609375 to 1.8984375
- gate_proj: bfloat16 [2048, 512], P('fs', 'tp'), may hold values from -0.125 to 0.125
- value_proj: bfloat16 [2048, 512], P('fs', 'tp'), may hold values from -1 to 1
- layer_gain: bfloat16 [512], replicated, may hold values from 0.099609375 to 1.8984375
- layer_shift: bfloat16 [512], replicated, may hold values from -3 to 3
- mix_kernel: bfloat16 [4, 128, 128], replicated, may hold values from -0.5 to 0.5
- mix_offset: bfloat16 [4, 128], replicated, may hold values from -4 to 4
- out_proj: bfloat16 [2048, 512], P('fs', 'tp'), may hold values from -0.25 to 0.25
- ffn_gain: bfloat16 [2048], replicated, may hold values from 0.099609375 to 1.8984375
- ffn_gate: bfloat16 [2048, 5632], P('fs', 'tp'), may hold values from -0.125 to 0.125
- ffn_up: bfloat16 [2048, 5632], P('fs', 'tp'), may hold values from -0.125 to 0.125
- ffn_down: bfloat16 [2048, 5632], P('fs', 'tp'), may hold values from -0.078125 to 0.078125
Outputs:
- layer_out: bfloat16 [4096, 2048], P(('rep', 'fs', 'tp'))
All inputs are finite; a program needn't handle non-finite values.
Results may differ from a plain program's by a relative error of at most 0.015.
Values may be sent and summed in bfloat16 or wider, within the bound.
A program may use at most 64 MiB of HBM per device.

v0:
```python
import jax
import jax.numpy as jnp
from jax import lax
from jax.sharding import PartitionSpec as P

epsilon = 1e-06


def rms_norm(rows, gain):
    floats = rows.astype(jnp.float32)
    scale = lax.rsqrt(jnp.mean(floats * floats, axis=-1, keepdims=True) + epsilon)
    return (floats * scale * gain.astype(jnp.float32)).astype(jnp.bfloat16)


def contract_last(left, right):
    return lax.dot_general(
        left, right, (((1,), (1,)), ((), ())), preferred_element_type=jnp.float32
    )


def per_device(
    tokens,
    mix_gain,
    gate_proj,
    value_proj,
    layer_gain,
    layer_shift,
    mix_kernel,
    mix_offset,
    out_proj,
    ffn_gain,
    ffn_gate,
    ffn_up,
    ffn_down,
):
    normed = rms_norm(tokens, mix_gain)
    gate_rows, value_rows, out_rows = (
        lax.all_gather(gate_proj, "fs", axis=0, tiled=True),
        lax.all_gather(value_proj, "fs", axis=0, tiled=True),
        lax.all_gather(out_proj, "fs", axis=0, tiled=True),
    )
    mix_width = layer_gain.shape[0]
    groups = mix_kernel.shape[0]
    span_len = mix_kernel.shape[1]
    causal = jnp.tril(jnp.ones((span_len, span_len), dtype=bool))
    masked = jnp.where(causal[None], mix_kernel, jnp.zeros_like(mix_kernel))
    local_width = gate_rows.shape[1]
    first_col = lax.axis_index("tp") * local_width
    joined = jnp.concatenate([gate_rows, value_rows], axis=1)
    preact = jnp.dot(
        lax.all_gather(normed, "tp", axis=0, tiled=True), joined, preferred_element_type=jnp.float32
    )
    gate_u = jax.nn.gelu(preact[:, :local_width])
    activated = jax.nn.gelu(preact[:, local_width:])
    row_sum, squares = lax.psum(
        (jnp.sum(activated, axis=-1), jnp.sum(activated * activated, axis=-1)), "tp"
    )
    center = (row_sum / mix_width)[:, None]
    spread = (squares / mix_width)[:, None] - center * center
    gain_part = lax.dynamic_slice_in_dim(layer_gain, first_col, local_width).astype(jnp.float32)
    shift_part = lax.dynamic_slice_in_dim(layer_shift, first_col, local_width).astype(jnp.float32)
    values = ((activated - center) * lax.rsqrt(spread + epsilon) * gain_part + shift_part).astype(
        jnp.bfloat16
    )
    group_id = first_col // (mix_width // groups)
    kernel = lax.dynamic_index_in_dim(masked, group_id, 0, keepdims=False)
    offset = lax.dynamic_index_in_dim(mix_offset, group_id, 0, keepdims=False).astype(jnp.float32)
    mixing = jnp.einsum(
        "ts,nsc->ntc",
        kernel,
        values.reshape(-1, span_len, local_width),
        preferred_element_type=jnp.float32,
    )
    mixing = mixing + offset[None, :, None]
    gated_rows = (gate_u * mixing.reshape(gate_u.shape)).astype(jnp.bfloat16)
    mixer_out = lax.psum_scatter(
        contract_last(gated_rows, out_rows).astype(jnp.bfloat16),
        "tp",
        scatter_dimension=0,
        tiled=True,
    ).astype(jnp.float32)
    middle = (tokens.astype(jnp.float32) + mixer_out).astype(jnp.bfloat16)
    normed2 = rms_norm(middle, ffn_gain)
    gathered = lax.all_gather(normed2, "tp", axis=0, tiled=True)
    gate_pre = jnp.dot(
        gathered,
        lax.all_gather(ffn_gate, "fs", axis=0, tiled=True),
        preferred_element_type=jnp.float32,
    )
    up_pre = jnp.dot(
        gathered,
        lax.all_gather(ffn_up, "fs", axis=0, tiled=True),
        preferred_element_type=jnp.float32,
    )
    hidden = (jax.nn.silu(gate_pre) * up_pre).astype(jnp.bfloat16)
    partial_value = contract_last(hidden, lax.all_gather(ffn_down, "fs", axis=0, tiled=True))
    summed = lax.psum_scatter(
        partial_value.astype(jnp.bfloat16), "tp", scatter_dimension=0, tiled=True
    ).astype(jnp.float32)
    return (middle.astype(jnp.float32) + summed).astype(jnp.bfloat16)


def solution(mesh):
    placed = (
        P(("rep", "fs", "tp"), None),
        P(),
        P("fs", "tp"),
        P("fs", "tp"),
        P(),
        P(),
        P(),
        P(),
        P("fs", "tp"),
        P(),
        P("fs", "tp"),
        P("fs", "tp"),
        P("fs", "tp"),
    )
    return jax.shard_map(
        per_device,
        mesh=mesh,
        in_specs=placed,
        out_specs=P(("rep", "fs", "tp"), None),
        check_vma=False,
    )
```

profile of v0, /device:TPU:0, one launch (start us, length us, event | category | flops | bytes accessed | tf_op | source)
XLA Modules:
  0.0 472.7 jit_solution(3375747574779029369)
XLA Ops:
  7.4 0.7 convert_element_type.64
  8.1 1.2 fusion.1
  9.3 2.0 fusion.3
  11.4 0.0 reduce-scatter.3.cloned.1.call-start
  11.5 0.7 bitcast_convert_fusion
  12.2 0.8 dynamic-slice_convert_fusion
  12.9 17.6 %all_gather.25 = bf16[2048,128]{1,0:T(8,128)(2,1)S(1)} all-gather(bf16[512,128]{1,0:T(8,128)(2,1)} %param.15), channel_id=1, replica_groups=mesh['rep'=2,'fs'=4,'tp'=4] {'fs'}, dimensions={0}, use_global_device_ids=true | all-gather | bytes 655360 | tf_op jit(solution)/shard_map/all_gather | solution.py:38
  30.5 16.7 %all_gather.26 = bf16[2048,128]{1,0:T(8,128)(2,1)S(1)} all-gather(bf16[512,128]{1,0:T(8,128)(2,1)S(1)} %copy-done.2), channel_id=1, replica_groups=mesh['rep'=2,'fs'=4,'tp'=4] {'fs'}, dimensions={0}, use_global_device_ids=true | all-gather | bytes 655360 | tf_op jit(solution)/shard_map/all_gather | solution.py:39
  47.2 15.6 %all_gather.27 = bf16[2048,128]{1,0:T(8,128)(2,1)S(1)} all-gather(bf16[512,128]{1,0:T(8,128)(2,1)S(1)} %copy-done.3), channel_id=1, replica_groups=mesh['rep'=2,'fs'=4,'tp'=4] {'fs'}, dimensions={0}, use_global_device_ids=true | all-gather | bytes 655360 | tf_op jit(solution)/shard_map/all_gather | solution.py:40
  62.8 2.3 fusion.9
  65.2 0.2 fusion.37
  65.4 5.7 %all-reduce = (f32[512]{0:T(512)S(1)}, f32[512]{0:T(512)S(1)}) all-reduce(f32[512]{0:T(512)S(1)} %get-tuple-element.6, f32[512]{0:T(512)S(1)} %get-tuple-element.5), channel_id=1, replica_groups=mesh['rep'=2,'fs'=4,'tp'=4] {'tp'}, use_global_device_ids=true, to_apply=%region_4.5 | all-reduce | flops 1024 | bytes 8192 | tf_op jit(solution)/shard_map/psum | solution.py:55
  71.1 0.2 add_convert_fusion
  71.3 0.9 convolution_add_fusion
  72.2 0.1 fusion.21
  72.4 2.1 convolution_convert_fusion
  74.5 0.0 all-gather.10.cloned.1.call-start
  74.5 0.5 all-gather.10.cloned.1.call-update
  75.1 31.4 %reduce-scatter.3.cloned.1.call-done = bf16[128,2048]{1,0:T(8,128)(2,1)} async-done(((bf16[512,2048]{1,0:T(8,128)(2,1)}), bf16[128,2048]{1,0:T(8,128)(2,1)}) %reduce-scatter.3.cloned.1.call-update) | async-done | bytes 524304 | tf_op jit(solution)/shard_map/reduce_scatter | solution.py:76
  106.5 1.3 fusion.5
  107.8 2.0 fusion.7
  109.9 0.0 all-gather.12.cloned.1.call-start
  110.0 0.5 all-gather.12.cloned.1.call-update
  110.6 0.7 all-gather.14.cloned.1.call-update
  111.3 72.6 %all-gather.10.cloned.1.call-done = bf16[2048,1408]{1,0:T(8,128)(2,1)} async-done(((bf16[512,1408]{1,0:T(8,128)(2,1)}), bf16[2048,1408]{1,0:T(8,128)(2,1)}) %all-gather.10.cloned.1.call-update) | async-done | bytes 5767184 | tf_op jit(solution)/shard_map/all_gather | solution.py:87
  183.9 22.1 %all-gather.8.cloned.1.call-done = bf16[512,2048]{1,0:T(8,128)(2,1)} async-done(((bf16[128,2048]{1,0:T(8,128)(2,1)}), bf16[512,2048]{1,0:T(8,128)(2,1)}) %all-gather.8.cloned.1.call-update) | async-done | bytes 2097168 | tf_op jit(solution)/shard_map/all_gather | solution.py:84
  206.0 8.4 %fusion.38 = f32[512,1408]{1,0:T(8,128)} fusion(bf16[512,2048]{1,0:T(8,128)(2,1)} %all-gather.8.cloned.1.call-done, bf16[2048,1408]{1,0:T(8,128)(2,1)} %all-gather.10.cloned.1.call-done), kind=kOutput, calls=%fused_computation.60 | convolution fusion | flops 2952790016 | bytes 10747904 | tf_op jit(solution)/shard_map/dot_general | solution.py:85
  214.4 99.6 %all-gather.12.cloned.1.call-done = bf16[2048,1408]{1,0:T(8,128)(2,1)} async-done(((bf16[512,1408]{1,0:T(8,128)(2,1)}), bf16[2048,1408]{1,0:T(8,128)(2,1)}) %all-gather.12.cloned.1.call-update) | async-done | bytes 5767184 | tf_op jit(solution)/shard_map/all_gather | solution.py:92
  314.0 106.4 %all-gather.14.cloned.1.call-done = bf16[2048,1408]{1,0:T(8,128)(2,1)} async-done(((bf16[512,1408]{1,0:T(8,128)(2,1)}), bf16[2048,1408]{1,0:T(8,128)(2,1)}) %all-gather.14.cloned.1.call-update) | async-done | bytes 5767184 | tf_op jit(solution)/shard_map/all_gather | solution.py:96
  420.5 13.2 %convolution_convert_fusion.1 = bf16[512,2048]{1,0:T(8,128)(2,1)} fusion(bf16[2048,1408]{1,0:T(8,128)(2,1)} %all-gather.14.cloned.1.call-done, bf16[512,2048]{1,0:T(8,128)(2,1)S(1)} %copy-done.5, bf16[2048,1408]{1,0:T(8,128)(2,1)} %all-gather.12.cloned.1.call-done, f32[512,1408]{1,0:T(8,128)} %fusion.38), kind=kOutput, calls=%fused_computation.3 | convolution fusion | flops 5910953984 | bytes 18612224 | tf_op jit(solution)/shard_map/dot_general | solution.py:16
  433.7 29.6 %reduce-scatter.5.cloned.1.call-done = bf16[128,2048]{1,0:T(8,128)(2,1)} async-done(((bf16[512,2048]{1,0:T(8,128)(2,1)}), bf16[128,2048]{1,0:T(8,128)(2,1)}) %reduce-scatter.5.cloned.1.call-update) | async-done | bytes 524304 | tf_op jit(solution)/shard_map/reduce_scatter | solution.py:97
  463.3 2.1 fusion.8
  (26 shorter events, 0.3 us)
Async XLA Ops:
  7.4 23.2 %copy-start.2 = (bf16[512,128]{1,0:T(8,128)(2,1)S(1)}, bf16[512,128]{1,0:T(8,128)(2,1)}, u32[]{:S(2)}) copy-start(bf16[512,128]{1,0:T(8,128)(2,1)} %param.16) | copy-start | bytes 393220
  7.4 39.9 %copy-start.3 = (bf16[512,128]{1,0:T(8,128)(2,1)S(1)}, bf16[512,128]{1,0:T(8,128)(2,1)}, u32[]{:S(2)}) copy-start(bf16[512,128]{1,0:T(8,128)(2,1)} %param.21) | copy-start | bytes 393220
  7.4 55.5 %all-gather.6.cloned.1.call-start = ((), (), s32[]{:S(2)}) async-start(), calls=%async_computation.2 | async-start | bytes 2621440 | tf_op jit(solution)/shard_map/all_gather | solution.py:51
  11.4 95.1 %reduce-scatter.3.cloned.1.call-start = ((), (), s32[]{:S(2)}) async-start(), calls=%async_computation.3 | async-start | bytes 2621440 | tf_op jit(solution)/shard_map/reduce_scatter | solution.py:76
  72.3 2.7 copy-start.4
  72.4 34.2 %copy-start = (bf16[128,2048]{1,0:T(8,128)(2,1)S(1)}, bf16[128,2048]{1,0:T(8,128)(2,1)}, u32[]{:S(2)}) copy-start(bf16[128,2048]{1,0:T(8,128)(2,1)} %param.13) | copy-start | bytes 1572868
  74.5 109.4 %all-gather.10.cloned.1.call-start = ((), (), s32[]{:S(2)}) async-start(), calls=%async_computation.5 | async-start | bytes 7208960 | tf_op jit(solution)/shard_map/all_gather | solution.py:87
  75.0 131.0 %all-gather.8.cloned.1.call-start = ((), (), s32[]{:S(2)}) async-start(), calls=%async_computation.4 | async-start | bytes 2621440 | tf_op jit(solution)/shard_map/all_gather | solution.py:84
  109.9 204.1 %all-gather.12.cloned.1.call-start = ((), (), s32[]{:S(2)}) async-start(), calls=%async_computation.6 | async-start | bytes 7208960 | tf_op jit(solution)/shard_map/all_gather | solution.py:92
  110.5 310.0 %all-gather.14.cloned.1.call-start = ((), (), s32[]{:S(2)}) async-start(), calls=%async_computation.7 | async-start | bytes 7208960 | tf_op jit(solution)/shard_map/all_gather | solution.py:96
  111.2 352.1 %reduce-scatter.5.cloned.1.call-start = ((), (), s32[]{:S(2)}) async-start(), calls=%async_computation.8 | async-start | bytes 2621440 | tf_op jit(solution)/shard_map/reduce_scatter | solution.py:97
  206.0 214.5 %copy-start.5 = (bf16[512,2048]{1,0:T(8,128)(2,1)S(1)}, bf16[512,2048]{1,0:T(8,128)(2,1)}, u32[]{:S(2)}) copy-start(bf16[512,2048]{1,0:T(8,128)(2,1)} %all-gather.8.cloned.1.call-done) | copy-start | bytes 6291460
  214.4 248.9 %copy-start.1 = (bf16[128,2048]{1,0:T(8,128)(2,1)S(1)}, bf16[128,2048]{1,0:T(8,128)(2,1)}, u32[]{:S(2)}) copy-start(bf16[128,2048]{1,0:T(8,128)(2,1)} %reduce-scatter.3.cloned.1.call-done) | copy-start | bytes 1572868
Sparse Core Ops, SparseCore 0:
  11.5 25.2 all-gather.5
  74.6 31.9 reduce-scatter.2
  433.8 29.4 reduce-scatter.4
Sparse Core Ops, SparseCore 1:
  76.5 107.3 all-gather.9
  185.3 20.7 all-gather.7
  207.5 106.5 all-gather.11
  315.6 104.8 all-gather.13
where the time goes:
time: 473 us
  waiting for transfers between devices  364 us (77%)
  blocking collectives  55.5 us (12%)
  matrix products  26.9 us (6%)
  between operations  14.9 us (3%)
  other arithmetic  11.5 us (2%)
    all_gather x1, waiting for transfers between devices, per_device(): lax.all_gather(ffn_down, 'fs', axis=0, tiled=True)  106 us
    all_gather x1, waiting for transfers between devices, per_device(): lax.all_gather(ffn_up, 'fs', axis=0, tiled=True)  99.6 us
    all_gather x1, waiting for transfers between devices, per_device(): lax.all_gather(ffn_gate, 'fs', axis=0, tiled=True)  72.6 us
    reduce_scatter x1, waiting for transfers between devices, per_device(): lax.psum_scatter(contract_last(gated_rows, out_rows).astype(jnp.bfloat16)...  31.4 us
    reduce_scatter x1, waiting for transfers between devices, per_device(): lax.psum_scatter(partial_value.astype(jnp.bfloat16), 'tp', scatter_dimens...  29.6 us
    all_gather x1, waiting for transfers between devices, per_device(): gathered = lax.all_gather(normed2, 'tp', axis=0, tiled=True)  22.1 us
    all_gather x1, blocking collectives, per_device(): lax.all_gather(gate_proj, 'fs', axis=0, tiled=True)  17.6 us
    all_gather x1, blocking collectives, per_device(): lax.all_gather(value_proj, 'fs', axis=0, tiled=True)  16.7 us
  transfers between devices with their start and end apart: 7, of which 6 were waited for; matrix products, arithmetic and copies ran while one was open for 3% of the time, Pallas kernels for 0%

commit v1 on v0

--- a/solution.py
+++ b/solution.py
@@ -4,6 +4,18 @@
 from jax.sharding import PartitionSpec as P
 
 epsilon = 1e-06
+
+
+def ring_gather(value, axis, dim):
+    ways, here, step = (lax.axis_size(axis), lax.axis_index(axis), value.shape[dim])
+    shape = [n * ways if d == dim else n for d, n in enumerate(value.shape)]
+    full = lax.dynamic_update_slice_in_dim(
+        jnp.zeros(shape, value.dtype), value, here * step, axis=dim
+    )
+    for far in range(1, ways):
+        value = lax.ppermute(value, axis, [(d, (d + 1) % ways) for d in range(ways)])
+        full = lax.dynamic_update_slice_in_dim(full, value, (here - far) % ways * step, axis=dim)
+    return full
 
 
 def rms_norm(rows, gain):
@@ -87,11 +99,7 @@
         lax.all_gather(ffn_gate, "fs", axis=0, tiled=True),
         preferred_element_type=jnp.float32,
     )
-    up_pre = jnp.dot(
-        gathered,
-        lax.all_gather(ffn_up, "fs", axis=0, tiled=True),
-        preferred_element_type=jnp.float32,
-    )
+    up_pre = jnp.dot(gathered, ring_gather(ffn_up, "fs", 0), preferred_element_type=jnp.float32)
     hidden = (jax.nn.silu(gate_pre) * up_pre).astype(jnp.bfloat16)
     partial_value = contract_last(hidden, lax.all_gather(ffn_down, "fs", axis=0, tiled=True))
     summed = lax.psum_scatter(

time: 473 us -> 427 us (0.903)
  waiting for transfers between devices: 364 us -> 278 us
  starting transfers between devices: 0.26 us -> 28.6 us
  local copies, waits for them, and re-layouts: 0.03 us -> 10.7 us
    ppermute x0 -> x3, waiting for transfers between devices: none -> 159 us  [ring_gather(): lax.ppermute(value, axis, [(d, (d + 1) % ways) for d in range(ways)])]
    all_gather x1 -> x0, waiting for transfers between devices: 99.6 us -> none  [per_device(): lax.all_gather(ffn_up, 'fs', axis=0, tiled=True)]
    all_gather x1, waiting for transfers between devices: 72.6 us -> 0.01 us  [per_device(): lax.all_gather(ffn_gate, 'fs', axis=0, tiled=True)]
    all_gather x1, waiting for transfers between devices: 106 us -> 56.9 us  [per_device(): lax.all_gather(ffn_down, 'fs', axis=0, tiled=True)]
    ppermute x0 -> x3, starting transfers between devices: none -> 28.4 us  [ring_gather(): lax.ppermute(value, axis, [(d, (d + 1) % ways) for d in range(ways)])]
    all_gather x1, waiting for transfers between devices: 22.1 us -> 0.01 us  [per_device(): gathered = lax.all_gather(normed2, 'tp', axis=0, tiled=True)]
    dynamic_update_slice x0 -> x4, local copies, waits for them, and re-layouts: none -> 7.85 us  [the longest x3 6.58 us: ring_gather(): lax.dynamic_update_slice_in_dim(full, value, (here - far) % ways * step,...]
  transfers between devices with their start and end apart: 7 -> 9, of which waited for: 6 -> 6; matrix products, arithmetic and copies ran while one was open for 3% -> 6% of each run, Pallas kernels for 0% -> 0%
where the time goes in v1:
time: 427 us; the launch traced here: 426 us
  waiting for transfers between devices  278 us (65%)
  blocking collectives  55.5 us (13%)
  starting transfers between devices  28.6 us (7%)
  matrix products  26.9 us (6%)
  between operations  14.9 us (3%)
  other arithmetic  11.5 us (3%)
  local copies, waits for them, and re-layouts  10.7 us (3%)
    ppermute x3, waiting for transfers between devices, ring_gather(): lax.ppermute(value, axis, [(d, (d + 1) % ways) for d in range(ways)])  159 us
    all_gather x1, waiting for transfers between devices, per_device(): lax.all_gather(ffn_down, 'fs', axis=0, tiled=True)  56.9 us
    reduce_scatter x1, waiting for transfers between devices, per_device(): lax.psum_scatter(contract_last(gated_rows, out_rows).astype(jnp.bfloat16)...  31.4 us
    reduce_scatter x1, waiting for transfers between devices, per_device(): lax.psum_scatter(partial_value.astype(jnp.bfloat16), 'tp', scatter_dimens...  29.7 us
    ppermute x3, starting transfers between devices, ring_gather(): lax.ppermute(value, axis, [(d, (d + 1) % ways) for d in range(ways)])  28.4 us
    all_gather x1, blocking collectives, per_device(): lax.all_gather(gate_proj, 'fs', axis=0, tiled=True)  17.6 us
    all_gather x1, blocking collectives, per_device(): lax.all_gather(value_proj, 'fs', axis=0, tiled=True)  16.7 us
    all_gather x1, blocking collectives, per_device(): lax.all_gather(out_proj, 'fs', axis=0, tiled=True)  15.6 us
  transfers between devices with their start and end apart: 9, of which 6 were waited for; matrix products, arithmetic and copies ran while one was open for 6% of the time, Pallas kernels for 0%

profile of v1, /device:TPU:0, one launch (start us, length us, event | category | flops | bytes accessed | tf_op | source)
XLA Modules:
  0.0 426.1 jit_solution(9055909583803223131)
XLA Ops:
  7.4 0.7 convert_element_type.64
  8.1 1.2 fusion.1
  9.3 2.0 fusion.3
  11.5 0.7 fusion.35
  12.2 0.8 dynamic-slice_convert_fusion
  12.9 17.6 %all_gather.22 = bf16[2048,128]{1,0:T(8,128)(2,1)S(1)} all-gather(bf16[512,128]{1,0:T(8,128)(2,1)} %param.15), channel_id=1, replica_groups=mesh['rep'=2,'fs'=4,'tp'=4] {'fs'}, dimensions={0}, use_global_device_ids=true | all-gather | bytes 655360 | tf_op jit(solution)/shard_map/all_gather | solution.py:50
  30.5 16.7 %all_gather.23 = bf16[2048,128]{1,0:T(8,128)(2,1)S(1)} all-gather(bf16[512,128]{1,0:T(8,128)(2,1)S(1)} %copy-done.3), channel_id=1, replica_groups=mesh['rep'=2,'fs'=4,'tp'=4] {'fs'}, dimensions={0}, use_global_device_ids=true | all-gather | bytes 655360 | tf_op jit(solution)/shard_map/all_gather | solution.py:51
  47.2 15.6 %all_gather.24 = bf16[2048,128]{1,0:T(8,128)(2,1)S(1)} all-gather(bf16[512,128]{1,0:T(8,128)(2,1)S(1)} %copy-done.4), channel_id=1, replica_groups=mesh['rep'=2,'fs'=4,'tp'=4] {'fs'}, dimensions={0}, use_global_device_ids=true | all-gather | bytes 655360 | tf_op jit(solution)/shard_map/all_gather | solution.py:52
  62.8 2.3 fusion.9
  65.4 5.7 %all-reduce = (f32[512]{0:T(512)S(1)}, f32[512]{0:T(512)S(1)}) all-reduce(f32[512]{0:T(512)S(1)} %get-tuple-element.6, f32[512]{0:T(512)S(1)} %get-tuple-element.5), channel_id=1, replica_groups=mesh['rep'=2,'fs'=4,'tp'=4] {'tp'}, use_global_device_ids=true, to_apply=%region_4.5 | all-reduce | flops 1024 | bytes 8192 | tf_op jit(solution)/shard_map/psum | solution.py:67
  71.3 0.9 convolution_add_fusion
  72.4 2.0 convolution_convert_fusion
  74.5 0.5 all-gather.9.cloned.1.call-update
  75.1 31.4 %reduce-scatter.3.cloned.1.call-done = bf16[128,2048]{1,0:T(8,128)(2,1)} async-done(((bf16[512,2048]{1,0:T(8,128)(2,1)}), bf16[128,2048]{1,0:T(8,128)(2,1)}) %reduce-scatter.3.cloned.1.call-update) | async-done | bytes 524304 | tf_op jit(solution)/shard_map/reduce_scatter | solution.py:88
  106.5 1.3 fusion.5
  107.8 2.0 fusion.7
  109.9 0.5 all-gather.11.cloned.1.call-update
  110.5 1.5 collective-permute-start
  112.1 65.3 %collective-permute-done = bf16[512,1408]{1,0:T(8,128)(2,1)S(1)} collective-permute-done((bf16[512,1408]{1,0:T(8,128)(2,1)S(1)}, bf16[512,1408]{1,0:T(8,128)(2,1)S(1)}, u32[]{:S(2)}, u32[]{:S(2)}) %collective-permute-start) | collective-permute-done | bytes 1441824 | tf_op jit(solution)/shard_map/ppermute | solution.py:16
  177.4 26.8 %collective-permute-start.1 = (bf16[512,1408]{1,0:T(8,128)(2,1)S(1)}, bf16[512,1408]{1,0:T(8,128)(2,1)}, u32[]{:S(2)}, u32[]{:S(2)}) collective-permute-start(bf16[512,1408]{1,0:T(8,128)(2,1)S(1)} %collective-permute-done), channel_id=1, source_target_pairs={{0,4},{4,8},{8,12},{12,0},{1,5},{5,9},{9,13},{13,1},{2,6},{6,10},{... | collective-permute-start | bytes 4325384 | tf_op jit(solution)/shard_map/ppermute | solution.py:16
  204.2 41.2 %collective-permute-done.1 = bf16[512,1408]{1,0:T(8,128)(2,1)} collective-permute-done((bf16[512,1408]{1,0:T(8,128)(2,1)S(1)}, bf16[512,1408]{1,0:T(8,128)(2,1)}, u32[]{:S(2)}, u32[]{:S(2)}) %collective-permute-start.1) | collective-permute-done | bytes 1441824 | tf_op jit(solution)/shard_map/ppermute | solution.py:16
  245.4 2.9 broadcast_in_dim.16
  248.2 1.3 constant_dynamic-update-slice_fusion.3
  249.5 1.2 constant_dynamic-update-slice_fusion.2
  250.7 2.8 constant_dynamic-update-slice_fusion.1
  253.5 52.4 %collective-permute-done.2 = bf16[512,1408]{1,0:T(8,128)(2,1)} collective-permute-done((bf16[512,1408]{1,0:T(8,128)(2,1)}, bf16[512,1408]{1,0:T(8,128)(2,1)}, u32[]{:S(2)}, u32[]{:S(2)}) %collective-permute-start.2) | collective-permute-done | bytes 1441824 | tf_op jit(solution)/shard_map/ppermute | solution.py:16
  305.9 2.6 constant_dynamic-update-slice_fusion
  308.5 8.4 %fusion.40 = f32[512,1408]{1,0:T(8,128)} fusion(bf16[512,2048]{1,0:T(8,128)(2,1)} %all-gather.7.cloned.1.call-done, bf16[2048,1408]{1,0:T(8,128)(2,1)} %all-gather.9.cloned.1.call-done), kind=kOutput, calls=%fused_computation.66 | convolution fusion | flops 2952790016 | bytes 10747904 | tf_op jit(solution)/shard_map/dot_general | solution.py:97
  316.9 56.9 %all-gather.11.cloned.1.call-done = bf16[2048,1408]{1,0:T(8,128)(2,1)} async-done(((bf16[512,1408]{1,0:T(8,128)(2,1)}), bf16[2048,1408]{1,0:T(8,128)(2,1)}) %all-gather.11.cloned.1.call-update) | async-done | bytes 5767184 | tf_op jit(solution)/shard_map/all_gather | solution.py:104
  373.8 13.2 %convolution_convert_fusion.1 = bf16[512,2048]{1,0:T(8,128)(2,1)} fusion(bf16[2048,1408]{1,0:T(8,128)(2,1)} %all-gather.11.cloned.1.call-done, bf16[512,2048]{1,0:T(8,128)(2,1)S(1)} %copy-done.6, bf16[2048,1408]{1,0:T(8,128)(2,1)} %constant_dynamic-update-slice_fusion, f32[512,1408]{1,0:T(8,128)} %fusion.40), kind=kOutput, calls=%fused_computation.3 | convolution fusion | flops 5910953984 | bytes 18612224 | tf_op jit(solution)/shard_map/dot_general | solution.py:28
  387.0 29.7 %reduce-scatter.5.cloned.1.call-done = bf16[128,2048]{1,0:T(8,128)(2,1)} async-done(((bf16[512,2048]{1,0:T(8,128)(2,1)}), bf16[128,2048]{1,0:T(8,128)(2,1)}) %reduce-scatter.5.cloned.1.call-update) | async-done | bytes 524304 | tf_op jit(solution)/shard_map/reduce_scatter | solution.py:105
  416.7 2.1 fusion.8
  (36 shorter events, 0.9 us)
Async XLA Ops:
  7.4 23.2 %copy-start.3 = (bf16[512,128]{1,0:T(8,128)(2,1)S(1)}, bf16[512,128]{1,0:T(8,128)(2,1)}, u32[]{:S(2)}) copy-start(bf16[512,128]{1,0:T(8,128)(2,1)} %param.16) | copy-start | bytes 393220
  7.4 39.9 %copy-start.4 = (bf16[512,128]{1,0:T(8,128)(2,1)S(1)}, bf16[512,128]{1,0:T(8,128)(2,1)}, u32[]{:S(2)}) copy-start(bf16[512,128]{1,0:T(8,128)(2,1)} %param.21) | copy-start | bytes 393220
  7.4 55.5 %all-gather.5.cloned.1.call-start = ((), (), s32[]{:S(2)}) async-start(), calls=%async_computation.2 | async-start | bytes 2621440 | tf_op jit(solution)/shard_map/all_gather | solution.py:63
  11.4 95.1 %reduce-scatter.3.cloned.1.call-start = ((), (), s32[]{:S(2)}) async-start(), calls=%async_computation.3 | async-start | bytes 2621440 | tf_op jit(solution)/shard_map/reduce_scatter | solution.py:88
  72.3 2.7 copy-start.5
  72.3 34.2 %copy-start = (bf16[128,2048]{1,0:T(8,128)(2,1)S(1)}, bf16[128,2048]{1,0:T(8,128)(2,1)}, u32[]{:S(2)}) copy-start(bf16[128,2048]{1,0:T(8,128)(2,1)} %param.13) | copy-start | bytes 1572868
  74.4 36.1 %copy-start.2 = (bf16[512,1408]{1,0:T(8,128)(2,1)S(1)}, bf16[512,1408]{1,0:T(8,128)(2,1)}, u32[]{:S(2)}) copy-start(bf16[512,1408]{1,0:T(8,128)(2,1)} %param.24) | copy-start | bytes 4325380
  74.4 234.0 %all-gather.9.cloned.1.call-start = ((), (), s32[]{:S(2)}) async-start(), calls=%async_computation.5 | async-start | bytes 7208960 | tf_op jit(solution)/shard_map/all_gather | solution.py:99
  75.0 233.5 %all-gather.7.cloned.1.call-start = ((), (), s32[]{:S(2)}) async-start(), calls=%async_computation.4 | async-start | bytes 2621440 | tf_op jit(solution)/shard_map/all_gather | solution.py:96
  109.9 263.9 %all-gather.11.cloned.1.call-start = ((), (), s32[]{:S(2)}) async-start(), calls=%async_computation.6 | async-start | bytes 7208960 | tf_op jit(solution)/shard_map/all_gather | solution.py:104
  110.5 306.2 %reduce-scatter.5.cloned.1.call-start = ((), (), s32[]{:S(2)}) async-start(), calls=%async_computation.7 | async-start | bytes 2621440 | tf_op jit(solution)/shard_map/reduce_scatter | solution.py:105
  110.5 66.8 %collective-permute-start = (bf16[512,1408]{1,0:T(8,128)(2,1)S(1)}, bf16[512,1408]{1,0:T(8,128)(2,1)S(1)}, u32[]{:S(2)}, u32[]{:S(2)}) collective-permute-start(bf16[512,1408]{1,0:T(8,128)(2,1)S(1)} %copy-done.2), channel_id=1, source_target_pairs={{0,4},{4,8},{8,12},{12,0},{1,5},{5,9},{9,13},{13,1},{2,6},{6,10},{... | collective-permute-start | bytes 4325384 | tf_op jit(solution)/shard_map/ppermute | solution.py:16
  177.4 68.0 %collective-permute-start.1 = (bf16[512,1408]{1,0:T(8,128)(2,1)S(1)}, bf16[512,1408]{1,0:T(8,128)(2,1)}, u32[]{:S(2)}, u32[]{:S(2)}) collective-permute-start(bf16[512,1408]{1,0:T(8,128)(2,1)S(1)} %collective-permute-done), channel_id=1, source_target_pairs={{0,4},{4,8},{8,12},{12,0},{1,5},{5,9},{9,13},{13,1},{2,6},{6,10},{... | collective-permute-start | bytes 4325384 | tf_op jit(solution)/shard_map/ppermute | solution.py:16
  245.4 60.5 %collective-permute-start.2 = (bf16[512,1408]{1,0:T(8,128)(2,1)}, bf16[512,1408]{1,0:T(8,128)(2,1)}, u32[]{:S(2)}, u32[]{:S(2)}) collective-permute-start(bf16[512,1408]{1,0:T(8,128)(2,1)} %collective-permute-done.1), channel_id=1, source_target_pairs={{0,4},{4,8},{8,12},{12,0},{1,5},{5,9},{9,13},{13,1},{2,6},{6,10},{... | collective-permute-start | bytes 4325384 | tf_op jit(solution)/shard_map/ppermute | solution.py:16
  308.5 65.3 %copy-start.6 = (bf16[512,2048]{1,0:T(8,128)(2,1)S(1)}, bf16[512,2048]{1,0:T(8,128)(2,1)}, u32[]{:S(2)}) copy-start(bf16[512,2048]{1,0:T(8,128)(2,1)} %all-gather.7.cloned.1.call-done) | copy-start | bytes 6291460
  316.9 99.8 %copy-start.1 = (bf16[128,2048]{1,0:T(8,128)(2,1)S(1)}, bf16[128,2048]{1,0:T(8,128)(2,1)}, u32[]{:S(2)}) copy-start(bf16[128,2048]{1,0:T(8,128)(2,1)} %reduce-scatter.3.cloned.1.call-done) | copy-start | bytes 1572868
Sparse Core Ops, SparseCore 0:
  11.5 25.2 all-gather.4
  74.5 31.9 reduce-scatter.2
  387.1 29.4 reduce-scatter.4
Sparse Core Ops, SparseCore 1:
  76.5 141.8 all-gather.8
  219.8 22.0 all-gather.6
  243.3 130.4 all-gather.10
